TPU v7x, 32 devices: a whole 2x2x4 slice. The times are simulated.
32 devices in a mesh: grp: 2 (over x), kv: 4 (over z), tp: 4 (over y, core).
Axes of the slice: x: 2, y: 2, z: 4, core: 2. Of those that a mesh axis runs over, the one named last changes fastest.
Arguments:
- tokens: bfloat16 [16, 4096], P('grp', 'tp'), parts along dimension 0, may hold values from -50 to 50
- pre_gain: float32 [4096], P('tp'), may hold values from 0.1 to 1.9
- gate_first: bfloat16 [4096, 11264], P('tp', 'kv'), may hold values from -0.09375 to 0.09375
- up_first: bfloat16 [4096, 11264], P('tp', 'kv'), may hold values from -0.09375 to 0.09375
- down_first: bfloat16 [11264, 4096], P('kv', 'tp'), may hold values from -0.0546875 to 0.0546875
- mix_gain: float32 [4096], P('tp'), may hold values from 0.1 to 1.9
- query_w: bfloat16 [4096, 4096], P('tp', 'kv'), may hold values from -0.09375 to 0.09375
- key_w: bfloat16 [4096, 4096], P('tp', 'kv'), may hold values from -0.09375 to 0.09375
- value_w: bfloat16 [4096, 4096], P('tp', 'kv'), may hold values from -0.09375 to 0.09375
- forget_w: bfloat16 [4096, 32], P('tp'), may hold values from -0.09375 to 0.09375
- key_cache: bfloat16 [16, 1024, 4096], P('grp', 'tp', 'kv'), parts along dimension 0, may hold values from -800 to 800
- value_cache: bfloat16 [16, 1024, 4096], P('grp', 'tp', 'kv'), parts along dimension 0, may hold values from -6 to 6
- gate_cache: float32 [16, 32, 1024], P('grp', 'kv', 'tp'), parts along dimension 0, may hold values from -130 to 0, as said below
- lengths: int32 [16], P('grp'), parts along dimension 0, may hold values from 64 to 1024, as said below
- out_w: bfloat16 [4096, 4096], P('kv', 'tp'), may hold values from -0.09375 to 0.09375
- post_gain: float32 [4096], P('tp'), may hold values from 0.1 to 1.9
- gate_second: bfloat16 [4096, 11264], P('tp', 'kv'), may hold values from -0.09375 to 0.09375
- up_second: bfloat16 [4096, 11264], P('tp', 'kv'), may hold values from -0.09375 to 0.09375
- down_second: bfloat16 [11264, 4096], P('kv', 'tp'), may hold values from -0.0546875 to 0.0546875
Outputs:
- out: bfloat16 [16, 4096], P('grp', 'tp'), parts along dimension 0
There are 2 independent parts, one for each index of `grp`. A program takes and returns all parts, laid end to end along the dimension named above; an argument that names none is the same for every part. Nothing has to cross between parts.
Inputs may be any that keep to these rules, and one draw needn't show every extreme that they name: `lengths`: each sequence's count of live cache positions; one sequence has all 1024 in every draw. `gate_cache`: at a live position p of sequence b, the sum of the log forget values of positions p + 1 to lengths[b] - 1 (zero at the last live position); never positive; zero beyond the live positions.
All inputs are finite; a program needn't handle non-finite values.
Results may differ from a plain program's by a relative error of at most 0.015.
Values may be sent and summed in bfloat16 or wider, within the bound.
A program may use at most 128 MiB of HBM per device.

v0:
```python
import jax
import jax.numpy as jnp
from jax import lax
from jax.sharding import PartitionSpec as P

D = 4096
HEAD_DIM = 128
EPSILON = 1e-06
MASKED = -1e30


def half_step(tok_rows, gain_part, w_gate, w_up, w_down):
    widened = tok_rows.astype(jnp.float32)
    squares = jnp.sum(widened * widened, axis=1)
    weighted = (widened * gain_part).astype(jnp.bfloat16)
    gate_part = jnp.dot(weighted, w_gate, preferred_element_type=jnp.float32)
    up_part = jnp.dot(weighted, w_up, preferred_element_type=jnp.float32)
    gate_sum, up_sum, sq_total = (
        lax.psum(gate_part.astype(jnp.bfloat16), "tp").astype(jnp.float32),
        lax.psum(up_part.astype(jnp.bfloat16), "tp").astype(jnp.float32),
        lax.psum(squares.astype(jnp.bfloat16), "tp").astype(jnp.float32),
    )
    norm_scale = lax.rsqrt(sq_total / D + EPSILON)[:, None]
    hidden = (jax.nn.silu(norm_scale * gate_sum) * (norm_scale * up_sum)).astype(jnp.bfloat16)
    down_part = jnp.dot(hidden, w_down, preferred_element_type=jnp.float32)
    down_sum = lax.psum(down_part, "kv")
    return (widened + 0.5 * down_sum).astype(jnp.bfloat16)


def absorb_parts(running, shard_part):
    run_top, run_mass, run_sum = running
    piece_top, masses, piece_sum = shard_part
    new_top = jnp.maximum(run_top, jnp.max(piece_top, axis=0))
    rescale = jnp.exp(run_top - new_top)
    factors = jnp.exp(piece_top - new_top[None])
    run_mass = run_mass * rescale + jnp.sum(masses * factors, axis=0)
    run_sum = run_sum * rescale[:, :, None] + jnp.sum(
        piece_sum.astype(jnp.float32) * factors[:, :, :, None], axis=0
    )
    return (new_top, run_mass, run_sum)


def attention(
    tok_rows,
    mix_gain,
    query_w,
    key_w,
    value_w,
    forget_w,
    key_cache,
    value_cache,
    gate_cache,
    lengths,
):
    widened = tok_rows.astype(jnp.float32)
    squares = jnp.sum(widened * widened, axis=1)
    weighted = (widened * mix_gain).astype(jnp.bfloat16)
    query_part = jnp.dot(weighted, query_w, preferred_element_type=jnp.float32)
    key_part = jnp.dot(weighted, key_w, preferred_element_type=jnp.float32)
    value_part = jnp.dot(weighted, value_w, preferred_element_type=jnp.float32)
    forget_part = jnp.dot(weighted, forget_w, preferred_element_type=jnp.float32)
    query_sum, key_sum, value_sum, forget_sum, sq_total = lax.psum(
        (query_part, key_part, value_part, forget_part, squares), "tp"
    )
    norm_scale = lax.rsqrt(sq_total / D + EPSILON)[:, None]
    query = (norm_scale * query_sum).astype(jnp.bfloat16)
    key_new = (norm_scale * key_sum).astype(jnp.bfloat16)
    value_new = (norm_scale * value_sum).astype(jnp.bfloat16)
    batch_rows = tok_rows.shape[0]
    heads_here = query.shape[1] // HEAD_DIM
    head_start = lax.axis_index("kv") * heads_here
    log_forget = jax.nn.log_sigmoid(
        norm_scale * lax.dynamic_slice_in_dim(forget_sum, head_start, heads_here, 1)
    )
    cache_span = key_cache.shape[1]
    query_heads = query.reshape(batch_rows, heads_here, HEAD_DIM)
    key_block = key_cache.reshape(batch_rows, cache_span, heads_here, HEAD_DIM)
    value_block = value_cache.reshape(batch_rows, cache_span, heads_here, HEAD_DIM)
    scores = jnp.einsum(
        "bhd,bphd->bhp", query_heads, key_block, preferred_element_type=jnp.float32
    ) * HEAD_DIM ** (-0.5)
    scores = scores + gate_cache + log_forget[:, :, None]
    slot_positions = lax.axis_index("tp") * cache_span + lax.iota(jnp.int32, cache_span)
    is_live = slot_positions[None, None, :] < lengths[:, None, None]
    local_top = jnp.max(jnp.where(is_live, scores, MASKED), axis=2)
    local_probs = jnp.where(is_live, jnp.exp(scores - local_top[:, :, None]), 0.0)
    local_mass = jnp.sum(local_probs, axis=2)
    local_sum = jnp.einsum(
        "bhp,bphd->bhd",
        local_probs.astype(jnp.bfloat16),
        value_block,
        preferred_element_type=jnp.float32,
    ).astype(jnp.bfloat16)
    initial = (
        jnp.full((batch_rows, heads_here), MASKED, jnp.float32),
        jnp.zeros((batch_rows, heads_here), jnp.float32),
        jnp.zeros((batch_rows, heads_here, HEAD_DIM), jnp.float32),
    )
    run_top, run_mass, run_sum = absorb_parts(
        initial,
        (
            lax.all_gather(local_top[None].astype(jnp.bfloat16), "tp", axis=0, tiled=True).astype(
                jnp.float32
            ),
            lax.all_gather(local_mass[None].astype(jnp.bfloat16), "tp", axis=0, tiled=True).astype(
                jnp.float32
            ),
            lax.all_gather(local_sum[None], "tp", axis=0, tiled=True),
        ),
    )
    new_heads = key_new.reshape(batch_rows, heads_here, HEAD_DIM).astype(jnp.float32)
    own_score = jnp.sum(query_heads.astype(jnp.float32) * new_heads, axis=2) * HEAD_DIM ** (-0.5)
    highest = jnp.maximum(run_top, own_score)
    rescale = jnp.exp(run_top - highest)
    own_weight = jnp.exp(own_score - highest)
    own_values = value_new.reshape(batch_rows, heads_here, HEAD_DIM).astype(jnp.float32)
    numer = run_sum * rescale[:, :, None] + own_weight[:, :, None] * own_values
    denom = run_mass * rescale + own_weight
    return (
        (numer / denom[:, :, None]).astype(jnp.bfloat16).reshape(batch_rows, heads_here * HEAD_DIM)
    )


def on_device(
    tokens,
    pre_gain,
    gate_first,
    up_first,
    down_first,
    mix_gain,
    query_w,
    key_w,
    value_w,
    forget_w,
    key_cache,
    value_cache,
    gate_cache,
    lengths,
    out_w,
    post_gain,
    gate_second,
    up_second,
    down_second,
):
    after_first = half_step(tokens, pre_gain, gate_first, up_first, down_first)
    attended = attention(
        after_first,
        mix_gain,
        query_w,
        key_w,
        value_w,
        forget_w,
        key_cache,
        value_cache,
        gate_cache,
        lengths,
    )
    projected = lax.psum(jnp.dot(attended, out_w, preferred_element_type=jnp.float32), "kv")
    residual_two = (after_first.astype(jnp.float32) + projected).astype(jnp.bfloat16)
    return half_step(residual_two, post_gain, gate_second, up_second, down_second)


def solution(mesh):
    placed = (
        P("grp", "tp"),
        P("tp"),
        P("tp", "kv"),
        P("tp", "kv"),
        P("kv", "tp"),
        P("tp"),
        P("tp", "kv"),
        P("tp", "kv"),
        P("tp", "kv"),
        P("tp", None),
        P("grp", "tp", "kv"),
        P("grp", "tp", "kv"),
        P("grp", "kv", "tp"),
        P("grp"),
        P("kv", "tp"),
        P("tp"),
        P("tp", "kv"),
        P("tp", "kv"),
        P("kv", "tp"),
    )
    return jax.shard_map(
        on_device, mesh=mesh, in_specs=placed, out_specs=P("grp", "tp"), check_vma=False
    )
```

profile of v0, /device:TPU:0, one launch (start us, length us, event | category | flops | bytes accessed | tf_op | source)
XLA Modules:
  0.0 220.3 jit_solution(18089456365356496139)
XLA Ops:
  6.6 1.5 fusion.15
  8.1 4.5 %convolution_convert_fusion.3 = bf16[8,2816]{1,0:T(8,128)(2,1)} fusion(bf16[1024,2816]{1,0:T(8,128)(2,1)} %param.21, bf16[8,1024]{1,0:T(8,128)(2,1)} %param.19, f32[1024]{0:T(1024)} %param.20), kind=kOutput, calls=%fused_computation.6 | convolution fusion | flops 46184448 | bytes 5832704 | tf_op jit(solution)/shard_map/dot_general | solution.py:16
  12.6 1.5 convolution_convert_fusion.2
  14.1 33.9 %all-reduce.11.cloned.1.call-done = (bf16[8,2816]{1,0:T(8,128)(2,1)}, bf16[8,2816]{1,0:T(8,128)(2,1)}, bf16[8]{0:T(256)(128)(2,1)}) async-done(((bf16[8,2816]{1,0:T(8,128)(2,1)}, bf16[8,2816]{1,0:T(8,128)(2,1)}, bf16[8]{0:T(256)(128)(2,1)}), (bf16[8,2816]{1,0:T(8,128)(2,1)}, bf16[8,2816]{1,0:T(8,128)(2,1)}, bf16[8]{0:T(256)(128)(2,1)})) %all-reduce.11.cloned.1.call-update) | async-done | bytes 90144 | tf_op jit(solution)/shard_map/psum | solution.py:20
  48.1 0.7 add_rsqrt_fusion.2
  48.7 3.6 %fusion.9 = f32[8,1024]{1,0:T(8,128)S(1)} fusion(bf16[2816,1024]{1,0:T(8,128)(2,1)} %param.23, bf16[8,2816]{1,0:T(8,128)(2,1)} %get-tuple-element.13, bf16[8,2816]{1,0:T(8,128)(2,1)} %get-tuple-element.14, f32[8]{0:T(128)S(1)} %add_rsqrt_fusion.2), kind=kOutput, calls=%fused_computation.28 | convolution fusion | flops 46362624 | bytes 5890080 | tf_op jit(solution)/shard_map/dot_general | solution.py:25
  52.3 19.1 %psum.101 = f32[8,1024]{1,0:T(8,128)S(1)} all-reduce(f32[8,1024]{1,0:T(8,128)S(1)} %fusion.9), channel_id=1, replica_groups=mesh['grp'=2,'kv'=4,'tp'=4] {'kv'}, use_global_device_ids=true, to_apply=%region_4.5 | all-reduce | flops 8192 | bytes 65536 | tf_op jit(solution)/shard_map/psum | solution.py:26
  71.4 0.7 fusion.18
  72.2 0.7 fusion.45
  72.9 1.0 fusion.43
  73.9 2.6 %fusion.41 = f32[8,1024]{1,0:T(8,128)} fusion(bf16[1024,1024]{1,0:T(8,128)(2,1)} %param.27, bf16[8,1024]{1,0:T(8,128)(2,1)S(1)} %get-tuple-element.21, f32[1024]{0:T(1024)S(1)} %copy-done.5), kind=kOutput, calls=%fused_computation.68 | convolution fusion | flops 16801792 | bytes 2150400 | tf_op jit(solution)/shard_map/dot_general | solution.py:60
  76.4 1.0 fusion.47
  77.6 6.4 %copy.38 = bf16[8,256,1024]{1,2,0:T(8,128)(2,1)} copy(bf16[8,256,1024]{2,1,0:T(8,128)(2,1)} %param.29) | data formatting | bytes 8388608 | tf_op jit(solution)/shard_map/reshape | solution.py:77
  84.0 21.8 %all-reduce.7.cloned.1.call-done = (f32[8,1024]{1,0:T(8,128)}, f32[8]{0:T(128)}, f32[8,32]{1,0:T(8,128)}, f32[8,1024]{1,0:T(8,128)}, f32[8,1024]{1,0:T(8,128)}) async-done(((f32[8,1024]{1,0:T(8,128)}, f32[8]{0:T(128)}, f32[8,32]{1,0:T(8,128)}, f32[8,1024]{1,0:T(8,128)}, f32[8,1024]{1,0:T(8,128)}), (f32[8,1024]{1,0:T(8,128)}, f32[8]{0:T(128)}, f32[8,32]{1,0:T(8,128)}, f32[8,1024]{1,0:T(8,128)}, ...) | async-done | bytes 99376 | tf_op jit(solution)/shard_map/psum | solution.py:62
  105.8 0.7 add_rsqrt_fusion.1
  106.5 0.8 fusion.54
  107.4 0.9 fusion.27
  108.4 0.8 fusion.51
  109.1 2.8 %fusion.28 = f32[8,8,1,256]{3,2,1,0:T(1,128)S(1)} fusion(bf16[8,256,8,128]{1,3,2,0:T(8,128)(2,1)} %bitcast.68, bf16[8,8,128,1]{2,0,1,3:T(8,128)(2,1)S(1)} %fusion.54), kind=kOutput, calls=%fused_computation.50 | convolution fusion | flops 4194304 | bytes 4276224 | tf_op jit(solution)/shard_map/bhd,bphd->bhp/dot_general | solution.py:79
  112.3 5.2 %all-gather = bf16[32,8]{1,0:T(8,128)(2,1)S(1)} all-gather(bf16[8,8]{1,0:T(8,128)(2,1)S(1)} %convert_element_type.152), channel_id=2, replica_groups=mesh['grp'=2,'kv'=4,'tp'=4] {'tp'}, dimensions={0}, use_global_device_ids=true | all-gather | bytes 640 | tf_op jit(solution)/shard_map/all_gather | solution.py:102
  117.6 5.5 %all-gather.2 = bf16[32,8]{1,0:T(8,128)(2,1)S(1)} all-gather(bf16[8,8]{1,0:T(8,128)(2,1)S(1)} %get-tuple-element.22), channel_id=4, replica_groups=mesh['grp'=2,'kv'=4,'tp'=4] {'tp'}, dimensions={0}, use_global_device_ids=true | all-gather | bytes 640 | tf_op jit(solution)/shard_map/all_gather | solution.py:105
  123.2 3.0 %fusion = f32[8,8,1,128]{3,2,1,0:T(1,128)S(1)} fusion(bf16[8,8,256,1]{2,1,0,3:T(8,128)(2,1)S(1)} %get-tuple-element.23, bf16[8,256,1024]{2,1,0:T(8,128)(2,1)} %param.30), kind=kOutput, calls=%fused_computation | convolution fusion | flops 4194304 | bytes 4259840 | tf_op jit(solution)/shard_map/bhp,bphd->bhd/dot_general | solution.py:88
  126.2 5.2 %all-gather.1 = bf16[32,8,128]{2,1,0:T(8,128)(2,1)S(1)} all-gather(bf16[8,8,128]{2,1,0:T(8,128)(2,1)S(1)} %convert_element_type.155), channel_id=3, replica_groups=mesh['grp'=2,'kv'=4,'tp'=4] {'tp'}, dimensions={0}, use_global_device_ids=true | all-gather | bytes 81920 | tf_op jit(solution)/shard_map/all_gather | solution.py:108
  132.1 19.3 %psum.107 = f32[8,1024]{1,0:T(8,128)S(1)} all-reduce(f32[8,1024]{1,0:T(8,128)S(1)} %fusion.31), channel_id=1, replica_groups=mesh['grp'=2,'kv'=4,'tp'=4] {'kv'}, use_global_device_ids=true, to_apply=%region_17.18 | all-reduce | flops 8192 | bytes 65536 | tf_op jit(solution)/shard_map/psum | solution.py:158
  151.4 0.6 fusion.21
  152.1 4.1 %convolution_convert_fusion.1 = bf16[8,2816]{1,0:T(8,128)(2,1)} fusion(bf16[1024,2816]{1,0:T(8,128)(2,1)} %param.35, bf16[8,1024]{1,0:T(8,128)(2,1)S(1)} %get-tuple-element.17, f32[1024]{0:T(1024)S(1)} %copy-done.10), kind=kOutput, calls=%fused_computation.4 | convolution fusion | flops 46184448 | bytes 5832704 | tf_op jit(solution)/shard_map/dot_general | solution.py:16
  156.2 4.1 %convolution_convert_fusion = bf16[8,2816]{1,0:T(8,128)(2,1)} fusion(bf16[1024,2816]{1,0:T(8,128)(2,1)} %param.36, bf16[8,1024]{1,0:T(8,128)(2,1)S(1)} %get-tuple-element.17, f32[1024]{0:T(1024)S(1)} %copy-done.10), kind=kOutput, calls=%fused_computation.3 | convolution fusion | flops 46184448 | bytes 5832704 | tf_op jit(solution)/shard_map/dot_general | solution.py:17
  160.3 29.6 %all-reduce.9.cloned.1.call-done = (bf16[8,2816]{1,0:T(8,128)(2,1)}, bf16[8,2816]{1,0:T(8,128)(2,1)}, bf16[8]{0:T(256)(128)(2,1)}) async-done(((bf16[8,2816]{1,0:T(8,128)(2,1)}, bf16[8,2816]{1,0:T(8,128)(2,1)}, bf16[8]{0:T(256)(128)(2,1)}), (bf16[8,2816]{1,0:T(8,128)(2,1)}, bf16[8,2816]{1,0:T(8,128)(2,1)}, bf16[8]{0:T(256)(128)(2,1)})) %all-reduce.9.cloned.1.call-update) | async-done | bytes 90144 | tf_op jit(solution)/shard_map/psum | solution.py:20
  190.0 0.7 add_rsqrt_fusion
  190.6 3.6 %fusion.10 = f32[8,1024]{1,0:T(8,128)S(1)} fusion(bf16[2816,1024]{1,0:T(8,128)(2,1)} %param.37, bf16[8,2816]{1,0:T(8,128)(2,1)} %get-tuple-element.10, bf16[8,2816]{1,0:T(8,128)(2,1)} %get-tuple-element.11, f32[8]{0:T(128)S(1)} %add_rsqrt_fusion), kind=kOutput, calls=%fused_computation.29 | convolution fusion | flops 46362624 | bytes 5890080 | tf_op jit(solution)/shard_map/dot_general | solution.py:25
  194.2 19.0 %psum.111 = f32[8,1024]{1,0:T(8,128)S(1)} all-reduce(f32[8,1024]{1,0:T(8,128)S(1)} %fusion.10), channel_id=1, replica_groups=mesh['grp'=2,'kv'=4,'tp'=4] {'kv'}, use_global_device_ids=true, to_apply=%region_22.23 | all-reduce | flops 8192 | bytes 65536 | tf_op jit(solution)/shard_map/psum | solution.py:26
  213.2 0.6 fusion.23
  (46 shorter events, 1.5 us)
Async XLA Ops:
  6.5 66.3 %copy-start = (bf16[1024,1024]{1,0:T(8,128)(2,1)S(1)}, bf16[1024,1024]{1,0:T(8,128)(2,1)}, u32[]{:S(2)}) copy-start(bf16[1024,1024]{1,0:T(8,128)(2,1)} %param.26) | copy-start | bytes 6291460
  6.5 6.0 %copy-start.4 = (bf16[8,1024]{1,0:T(8,128)(2,1)S(1)}, bf16[8,1024]{1,0:T(8,128)(2,1)}, u32[]{:S(2)}) copy-start(bf16[8,1024]{1,0:T(8,128)(2,1)} %param.19) | copy-start | bytes 49156
  6.5 6.0 %copy-start.9 = (f32[1024]{0:T(1024)S(1)}, f32[1024]{0:T(1024)}, u32[]{:S(2)}) copy-start(f32[1024]{0:T(1024)} %param.20) | copy-start | bytes 12292
  6.5 41.5 %all-reduce.11.cloned.1.call-start = ((), (), s32[]{:S(2)}) async-start(), calls=%async_computation.2 | async-start | bytes 181248 | tf_op jit(solution)/shard_map/psum | solution.py:20
  6.5 6.0 %copy-start.1 = (bf16[1024,2816]{1,0:T(8,128)(2,1)S(1)}, bf16[1024,2816]{1,0:T(8,128)(2,1)}, u32[]{:S(2)}) copy-start(bf16[1024,2816]{1,0:T(8,128)(2,1)} %param.22) | copy-start | bytes 17301508
  14.0 58.1 %copy-start.5 = (f32[1024]{0:T(1024)S(1)}, f32[1024]{0:T(1024)}, u32[]{:S(2)}) copy-start(f32[1024]{0:T(1024)} %param.24) | copy-start | bytes 12292
  14.0 58.1 %copy-start.7 = (bf16[1024,32]{0,1:T(8,128)(2,1)S(1)}, bf16[1024,32]{0,1:T(8,128)(2,1)}, u32[]{:S(2)}) copy-start(bf16[1024,32]{0,1:T(8,128)(2,1)} %param.28) | copy-start | bytes 196612
  14.1 91.8 %all-reduce.7.cloned.1.call-start = ((), (), s32[]{:S(2)}) async-start(), calls=%async_computation | async-start | bytes 205824 | tf_op jit(solution)/shard_map/psum | solution.py:62
  52.3 25.2 %copy-start.11 = (s32[8]{0:T(128)S(1)}, s32[8]{0:T(128)}, u32[]{:S(2)}) copy-start(s32[8]{0:T(128)} %param.32) | copy-start | bytes 100
  71.4 5.0 %copy-start.3 = (bf16[1024,1024]{1,0:T(8,128)(2,1)S(1)}, bf16[1024,1024]{1,0:T(8,128)(2,1)}, u32[]{:S(2)}) copy-start(bf16[1024,1024]{1,0:T(8,128)(2,1)} %param.25) | copy-start | bytes 6291460
  77.5 112.5 %all-reduce.9.cloned.1.call-start = ((), (), s32[]{:S(2)}) async-start(), calls=%async_computation.1 | async-start | bytes 181248 | tf_op jit(solution)/shard_map/psum | solution.py:20
  84.0 28.0 %copy-start.6 = (f32[8,8,256]{2,1,0:T(8,128)S(1)}, f32[8,8,256]{2,1,0:T(8,128)}, u32[]{:S(2)}) copy-start(f32[8,8,256]{2,1,0:T(8,128)} %param.31) | copy-start | bytes 196612
  109.1 22.5 %copy-start.8 = (f32[8,1024]{1,0:T(8,128)S(1)}, f32[8,1024]{1,0:T(8,128)}, u32[]{:S(2)}) copy-start(f32[8,1024]{1,0:T(8,128)} %get-tuple-element.9) | copy-start | bytes 98308
  112.0 40.1 %copy-start.10 = (f32[1024]{0:T(1024)S(1)}, f32[1024]{0:T(1024)}, u32[]{:S(2)}) copy-start(f32[1024]{0:T(1024)} %param.34) | copy-start | bytes 12292
  123.2 8.4 %copy-start.2 = (bf16[1024,1024]{1,0:T(8,128)(2,1)S(1)}, bf16[1024,1024]{1,0:T(8,128)(2,1)}, u32[]{:S(2)}) copy-start(bf16[1024,1024]{1,0:T(8,128)(2,1)} %param.33) | copy-start | bytes 6291460
Sparse Core Ops, SparseCore 0:
  14.2 33.8 all-reduce.10
  77.6 28.2 all-reduce.6
  160.4 29.4 all-reduce.8
where the time goes:
time: 221 us; the launch traced here: 220 us
  waiting for transfers between devices  85.4 us (39%)
  blocking collectives  73.4 us (33%)
  matrix products  32.9 us (15%)
  between operations  13.3 us (6%)
  other arithmetic  8.63 us (4%)
  local copies, waits for them, and re-layouts  6.69 us (3%)
    psum x2, waiting for transfers between devices, half_step(): lax.psum(up_part.astype(jnp.bfloat16), 'tp').astype(jnp.float32)  63.5 us
    psum x2, blocking collectives, half_step(): down_sum = lax.psum(down_part, 'kv')  38.1 us
    psum x1, waiting for transfers between devices, attention(): lax.psum((query_part, key_part, value_part, forget_part, squares), 'tp')  21.8 us
    psum x1, blocking collectives, on_device(): lax.psum(jnp.dot(attended, out_w, preferred_element_type=jnp.float32), 'kv')  19.3 us
    dot_general x2, matrix products, half_step(): gate_part = jnp.dot(weighted, w_gate, preferred_element_type=jnp.float32)  8.61 us
    dot_general x2, matrix products, half_step(): down_part = jnp.dot(hidden, w_down, preferred_element_type=jnp.float32)  7.18 us
    reshape x1, local copies, waits for them, and re-layouts, attention(): key_block = key_cache.reshape(batch_rows, cache_span, heads_here, HEAD_DIM)  6.44 us
    dot_general x2, matrix products, half_step(): up_part = jnp.dot(weighted, w_up, preferred_element_type=jnp.float32)  5.58 us
  transfers between devices with their start and end apart: 3, of which 3 were waited for; matrix products, arithmetic and copies ran while one was open for 3% of the time, Pallas kernels for 0%

commit v1 on v0

--- a/solution.py
+++ b/solution.py
@@ -23,7 +23,7 @@
     norm_scale = lax.rsqrt(sq_total / D + EPSILON)[:, None]
     hidden = (jax.nn.silu(norm_scale * gate_sum) * (norm_scale * up_sum)).astype(jnp.bfloat16)
     down_part = jnp.dot(hidden, w_down, preferred_element_type=jnp.float32)
-    down_sum = lax.psum(down_part, "kv")
+    down_sum = jnp.sum(lax.all_gather(down_part, "kv"), axis=0)
     return (widened + 0.5 * down_sum).astype(jnp.bfloat16)
 
 

time: 221 us -> 211 us (0.955)
  blocking collectives: 73.4 us -> 62.2 us
  waiting for transfers between devices: 85.4 us -> 88.1 us
    psum x2 -> x0, blocking collectives: 38.1 us -> none  [half_step(): down_sum = lax.psum(down_part, 'kv')]
    all_gather x0 -> x2, blocking collectives: none -> 26.9 us  [half_step(): down_sum = jnp.sum(lax.all_gather(down_part, 'kv'), axis=0)]
    psum x1, waiting for transfers between devices: 21.8 us -> 24.5 us  [attention(): lax.psum((query_part, key_part, value_part, forget_part, squares), 'tp')]
where the time goes in v1:
time: 211 us; the launch traced here: 210 us
  waiting for transfers between devices  88.1 us (42%)
  blocking collectives  62.2 us (29%)
  matrix products  31.5 us (15%)
  between operations  13.2 us (6%)
  other arithmetic  8.65 us (4%)
  local copies, waits for them, and re-layouts  6.69 us (3%)
    psum x2, waiting for transfers between devices, half_step(): lax.psum(up_part.astype(jnp.bfloat16), 'tp').astype(jnp.float32)  63.5 us
    all_gather x2, blocking collectives, half_step(): down_sum = jnp.sum(lax.all_gather(down_part, 'kv'), axis=0)  26.9 us
    psum x1, waiting for transfers between devices, attention(): lax.psum((query_part, key_part, value_part, forget_part, squares), 'tp')  24.5 us
    psum x1, blocking collectives, on_device(): lax.psum(jnp.dot(attended, out_w, preferred_element_type=jnp.float32), 'kv')  19.3 us
    dot_general x2, matrix products, half_step(): gate_part = jnp.dot(weighted, w_gate, preferred_element_type=jnp.float32)  8.61 us
    dot_general x2, matrix products, half_step(): down_part = jnp.dot(hidden, w_down, preferred_element_type=jnp.float32)  7.33 us
    reshape x1, local copies, waits for them, and re-layouts, attention(): key_block = key_cache.reshape(batch_rows, cache_span, heads_here, HEAD_DIM)  6.43 us
    dot_general x2, matrix products, half_step(): up_part = jnp.dot(weighted, w_up, preferred_element_type=jnp.float32)  5.58 us
  transfers between devices with their start and end apart: 3, of which 3 were waited for; matrix products, arithmetic and copies ran while one was open for 3% of the time, Pallas kernels for 0%

profile of v1, /device:TPU:0, one launch (start us, length us, event | category | flops | bytes accessed | tf_op | source)
XLA Modules:
  0.0 210.5 jit_solution(5156036471447752741)
XLA Ops:
  6.6 1.5 fusion.15
  8.1 4.5 %convolution_convert_fusion.3 = bf16[8,2816]{1,0:T(8,128)(2,1)} fusion(bf16[1024,2816]{1,0:T(8,128)(2,1)} %param.21, bf16[8,1024]{1,0:T(8,128)(2,1)} %param.19, f32[1024]{0:T(1024)} %param.20), kind=kOutput, calls=%fused_computation.6 | convolution fusion | flops 46184448 | bytes 5832704 | tf_op jit(solution)/shard_map/dot_general | solution.py:16
  12.6 1.5 convolution_convert_fusion.2
  14.1 33.9 %all-reduce.11.cloned.1.call-done = (bf16[8,2816]{1,0:T(8,128)(2,1)}, bf16[8,2816]{1,0:T(8,128)(2,1)}, bf16[8]{0:T(256)(128)(2,1)}) async-done(((bf16[8,2816]{1,0:T(8,128)(2,1)}, bf16[8,2816]{1,0:T(8,128)(2,1)}, bf16[8]{0:T(256)(128)(2,1)}), (bf16[8,2816]{1,0:T(8,128)(2,1)}, bf16[8,2816]{1,0:T(8,128)(2,1)}, bf16[8]{0:T(256)(128)(2,1)})) %all-reduce.11.cloned.1.call-update) | async-done | bytes 90144 | tf_op jit(solution)/shard_map/psum | solution.py:20
  48.1 0.7 add_rsqrt_fusion.2
  48.7 3.7 %fusion.9 = f32[8,1024]{1,0:T(8,128)S(1)} fusion(bf16[2816,1024]{1,0:T(8,128)(2,1)} %param.23, bf16[8,2816]{1,0:T(8,128)(2,1)} %get-tuple-element.13, bf16[8,2816]{1,0:T(8,128)(2,1)} %get-tuple-element.14, f32[8]{0:T(128)S(1)} %add_rsqrt_fusion.2), kind=kOutput, calls=%fused_computation.30 | convolution fusion | flops 46362624 | bytes 5890080 | tf_op jit(solution)/shard_map/dot_general | solution.py:25
  52.5 13.5 %all-gather = f32[32,1024]{1,0:T(8,128)S(1)} all-gather(f32[8,1024]{1,0:T(8,128)S(1)} %fusion.9), channel_id=2, replica_groups=mesh['grp'=2,'kv'=4,'tp'=4] {'kv'}, dimensions={0}, use_global_device_ids=true | all-gather | bytes 163840 | tf_op jit(solution)/shard_map/all_gather | solution.py:26
  66.0 0.7 fusion.18
  66.7 0.7 fusion.45
  67.4 1.0 fusion.43
  68.4 1.0 fusion.41
  69.4 1.0 fusion.47
  70.6 6.4 %copy.38 = bf16[8,256,1024]{1,2,0:T(8,128)(2,1)} copy(bf16[8,256,1024]{2,1,0:T(8,128)(2,1)} %param.29) | data formatting | bytes 8388608 | tf_op jit(solution)/shard_map/reshape | solution.py:77
  77.0 24.5 %all-reduce.7.cloned.1.call-done = (f32[8,1024]{1,0:T(8,128)}, f32[8]{0:T(128)}, f32[8,32]{1,0:T(8,128)}, f32[8,1024]{1,0:T(8,128)}, f32[8,1024]{1,0:T(8,128)}) async-done(((f32[8,1024]{1,0:T(8,128)}, f32[8]{0:T(128)}, f32[8,32]{1,0:T(8,128)}, f32[8,1024]{1,0:T(8,128)}, f32[8,1024]{1,0:T(8,128)}), (f32[8,1024]{1,0:T(8,128)}, f32[8]{0:T(128)}, f32[8,32]{1,0:T(8,128)}, f32[8,1024]{1,0:T(8,128)}, ...) | async-done | bytes 99376 | tf_op jit(solution)/shard_map/psum | solution.py:62
  101.5 0.7 add_rsqrt_fusion.1
  102.2 0.8 fusion.54
  103.1 0.9 fusion.27
  104.1 0.8 fusion.51
  104.8 2.8 %fusion.28 = f32[8,8,1,256]{3,2,1,0:T(1,128)S(1)} fusion(bf16[8,256,8,128]{1,3,2,0:T(8,128)(2,1)} %bitcast.72, bf16[8,8,128,1]{2,0,1,3:T(8,128)(2,1)S(1)} %fusion.54), kind=kOutput, calls=%fused_computation.52 | convolution fusion | flops 4194304 | bytes 4276224 | tf_op jit(solution)/shard_map/bhd,bphd->bhp/dot_general | solution.py:79
  108.0 5.2 %all-gather.1 = bf16[32,8]{1,0:T(8,128)(2,1)S(1)} all-gather(bf16[8,8]{1,0:T(8,128)(2,1)S(1)} %convert_element_type.152), channel_id=3, replica_groups=mesh['grp'=2,'kv'=4,'tp'=4] {'tp'}, dimensions={0}, use_global_device_ids=true | all-gather | bytes 640 | tf_op jit(solution)/shard_map/all_gather | solution.py:102
  113.3 5.5 %all-gather.3 = bf16[32,8]{1,0:T(8,128)(2,1)S(1)} all-gather(bf16[8,8]{1,0:T(8,128)(2,1)S(1)} %get-tuple-element.22), channel_id=5, replica_groups=mesh['grp'=2,'kv'=4,'tp'=4] {'tp'}, dimensions={0}, use_global_device_ids=true | all-gather | bytes 640 | tf_op jit(solution)/shard_map/all_gather | solution.py:105
  118.9 3.0 %fusion = f32[8,8,1,128]{3,2,1,0:T(1,128)S(1)} fusion(bf16[8,8,256,1]{2,1,0,3:T(8,128)(2,1)S(1)} %get-tuple-element.23, bf16[8,256,1024]{2,1,0:T(8,128)(2,1)} %param.30), kind=kOutput, calls=%fused_computation | convolution fusion | flops 4194304 | bytes 4259840 | tf_op jit(solution)/shard_map/bhp,bphd->bhd/dot_general | solution.py:88
  121.9 5.2 %all-gather.2 = bf16[32,8,128]{2,1,0:T(8,128)(2,1)S(1)} all-gather(bf16[8,8,128]{2,1,0:T(8,128)(2,1)S(1)} %convert_element_type.155), channel_id=4, replica_groups=mesh['grp'=2,'kv'=4,'tp'=4] {'tp'}, dimensions={0}, use_global_device_ids=true | all-gather | bytes 81920 | tf_op jit(solution)/shard_map/all_gather | solution.py:108
  127.8 19.3 %psum.92 = f32[8,1024]{1,0:T(8,128)S(1)} all-reduce(f32[8,1024]{1,0:T(8,128)S(1)} %fusion.31), channel_id=1, replica_groups=mesh['grp'=2,'kv'=4,'tp'=4] {'kv'}, use_global_device_ids=true, to_apply=%region_17.18 | all-reduce | flops 8192 | bytes 65536 | tf_op jit(solution)/shard_map/psum | solution.py:158
  147.2 0.6 fusion.21
  147.8 4.1 %convolution_convert_fusion.1 = bf16[8,2816]{1,0:T(8,128)(2,1)} fusion(bf16[1024,2816]{1,0:T(8,128)(2,1)} %param.35, bf16[8,1024]{1,0:T(8,128)(2,1)S(1)} %get-tuple-element.17, f32[1024]{0:T(1024)S(1)} %copy-done.11), kind=kOutput, calls=%fused_computation.4 | convolution fusion | flops 46184448 | bytes 5832704 | tf_op jit(solution)/shard_map/dot_general | solution.py:16
  151.9 4.1 %convolution_convert_fusion = bf16[8,2816]{1,0:T(8,128)(2,1)} fusion(bf16[1024,2816]{1,0:T(8,128)(2,1)} %param.36, bf16[8,1024]{1,0:T(8,128)(2,1)S(1)} %get-tuple-element.17, f32[1024]{0:T(1024)S(1)} %copy-done.11), kind=kOutput, calls=%fused_computation.3 | convolution fusion | flops 46184448 | bytes 5832704 | tf_op jit(solution)/shard_map/dot_general | solution.py:17
  156.0 29.6 %all-reduce.9.cloned.1.call-done = (bf16[8,2816]{1,0:T(8,128)(2,1)}, bf16[8,2816]{1,0:T(8,128)(2,1)}, bf16[8]{0:T(256)(128)(2,1)}) async-done(((bf16[8,2816]{1,0:T(8,128)(2,1)}, bf16[8,2816]{1,0:T(8,128)(2,1)}, bf16[8]{0:T(256)(128)(2,1)}), (bf16[8,2816]{1,0:T(8,128)(2,1)}, bf16[8,2816]{1,0:T(8,128)(2,1)}, bf16[8]{0:T(256)(128)(2,1)})) %all-reduce.9.cloned.1.call-update) | async-done | bytes 90144 | tf_op jit(solution)/shard_map/psum | solution.py:20
  185.7 0.7 add_rsqrt_fusion
  186.3 3.6 %fusion.10 = f32[8,1024]{1,0:T(8,128)S(1)} fusion(bf16[2816,1024]{1,0:T(8,128)(2,1)} %param.37, bf16[8,2816]{1,0:T(8,128)(2,1)} %get-tuple-element.10, bf16[8,2816]{1,0:T(8,128)(2,1)} %get-tuple-element.11, f32[8]{0:T(128)S(1)} %add_rsqrt_fusion), kind=kOutput, calls=%fused_computation.31 | convolution fusion | flops 46362624 | bytes 5890080 | tf_op jit(solution)/shard_map/dot_general | solution.py:25
  189.9 13.4 %all-gather.4 = f32[32,1024]{1,0:T(8,128)S(1)} all-gather(f32[8,1024]{1,0:T(8,128)S(1)} %fusion.10), channel_id=6, replica_groups=mesh['grp'=2,'kv'=4,'tp'=4] {'kv'}, dimensions={0}, use_global_device_ids=true | all-gather | bytes 163840 | tf_op jit(solution)/shard_map/all_gather | solution.py:26
  203.3 0.6 fusion.23
  (50 shorter events, 1.5 us)
Async XLA Ops:
  6.5 60.9 %copy-start = (bf16[1024,1024]{1,0:T(8,128)(2,1)S(1)}, bf16[1024,1024]{1,0:T(8,128)(2,1)}, u32[]{:S(2)}) copy-start(bf16[1024,1024]{1,0:T(8,128)(2,1)} %param.26) | copy-start | bytes 6291460
  6.5 6.0 %copy-start.5 = (bf16[8,1024]{1,0:T(8,128)(2,1)S(1)}, bf16[8,1024]{1,0:T(8,128)(2,1)}, u32[]{:S(2)}) copy-start(bf16[8,1024]{1,0:T(8,128)(2,1)} %param.19) | copy-start | bytes 49156
  6.5 6.0 %copy-start.10 = (f32[1024]{0:T(1024)S(1)}, f32[1024]{0:T(1024)}, u32[]{:S(2)}) copy-start(f32[1024]{0:T(1024)} %param.20) | copy-start | bytes 12292
  6.5 41.5 %all-reduce.11.cloned.1.call-start = ((), (), s32[]{:S(2)}) async-start(), calls=%async_computation.2 | async-start | bytes 181248 | tf_op jit(solution)/shard_map/psum | solution.py:20
  6.5 6.0 %copy-start.1 = (bf16[1024,2816]{1,0:T(8,128)(2,1)S(1)}, bf16[1024,2816]{1,0:T(8,128)(2,1)}, u32[]{:S(2)}) copy-start(bf16[1024,2816]{1,0:T(8,128)(2,1)} %param.22) | copy-start | bytes 17301508
  14.0 52.7 %copy-start.6 = (f32[1024]{0:T(1024)S(1)}, f32[1024]{0:T(1024)}, u32[]{:S(2)}) copy-start(f32[1024]{0:T(1024)} %param.24) | copy-start | bytes 12292
  14.0 52.7 %copy-start.8 = (bf16[1024,32]{0,1:T(8,128)(2,1)S(1)}, bf16[1024,32]{0,1:T(8,128)(2,1)}, u32[]{:S(2)}) copy-start(bf16[1024,32]{0,1:T(8,128)(2,1)} %param.28) | copy-start | bytes 196612
  14.1 87.5 %all-reduce.7.cloned.1.call-start = ((), (), s32[]{:S(2)}) async-start(), calls=%async_computation | async-start | bytes 205824 | tf_op jit(solution)/shard_map/psum | solution.py:62
  48.7 19.7 %copy-start.3 = (bf16[1024,1024]{1,0:T(8,128)(2,1)S(1)}, bf16[1024,1024]{1,0:T(8,128)(2,1)}, u32[]{:S(2)}) copy-start(bf16[1024,1024]{1,0:T(8,128)(2,1)} %param.27) | copy-start | bytes 6291460
  48.7 20.7 %copy-start.4 = (bf16[1024,1024]{1,0:T(8,128)(2,1)S(1)}, bf16[1024,1024]{1,0:T(8,128)(2,1)}, u32[]{:S(2)}) copy-start(bf16[1024,1024]{1,0:T(8,128)(2,1)} %param.25) | copy-start | bytes 6291460
  52.5 18.0 %copy-start.12 = (s32[8]{0:T(128)S(1)}, s32[8]{0:T(128)}, u32[]{:S(2)}) copy-start(s32[8]{0:T(128)} %param.32) | copy-start | bytes 100
  70.4 115.2 %all-reduce.9.cloned.1.call-start = ((), (), s32[]{:S(2)}) async-start(), calls=%async_computation.1 | async-start | bytes 181248 | tf_op jit(solution)/shard_map/psum | solution.py:20
  77.0 30.7 %copy-start.7 = (f32[8,8,256]{2,1,0:T(8,128)S(1)}, f32[8,8,256]{2,1,0:T(8,128)}, u32[]{:S(2)}) copy-start(f32[8,8,256]{2,1,0:T(8,128)} %param.31) | copy-start | bytes 196612
  104.8 22.5 %copy-start.9 = (f32[8,1024]{1,0:T(8,128)S(1)}, f32[8,1024]{1,0:T(8,128)}, u32[]{:S(2)}) copy-start(f32[8,1024]{1,0:T(8,128)} %get-tuple-element.9) | copy-start | bytes 98308
  107.7 40.1 %copy-start.11 = (f32[1024]{0:T(1024)S(1)}, f32[1024]{0:T(1024)}, u32[]{:S(2)}) copy-start(f32[1024]{0:T(1024)} %param.34) | copy-start | bytes 12292
  118.9 8.4 %copy-start.2 = (bf16[1024,1024]{1,0:T(8,128)(2,1)S(1)}, bf16[1024,1024]{1,0:T(8,128)(2,1)}, u32[]{:S(2)}) copy-start(bf16[1024,1024]{1,0:T(8,128)(2,1)} %param.33) | copy-start | bytes 6291460
Sparse Core Ops, SparseCore 0:
  14.2 33.8 all-reduce.10
  70.5 30.9 all-reduce.6
  156.1 29.4 all-reduce.8
